TPU v7x, 32 devices: a whole 2x2x4 slice. The times are simulated.
32 devices in a mesh: ep: 8 (over z, y), tp: 4 (over x, core).
Axes of the slice: x: 2, y: 2, z: 4, core: 2. Of those that a mesh axis runs over, the one named last changes fastest.
Arguments:
- query: bfloat16 [1024, 1536], P('ep', 'tp'), may hold values from -136 to 136
- latent: bfloat16 [1024, 512], P(('ep', 'tp')), may hold values from -6 to 6
- rope_key: bfloat16 [1024, 32], P(('ep', 'tp')), may hold values from -6 to 6
- latent_gain: float32 [512], replicated, may hold values from 0.1 to 1.9
- key_up: bfloat16 [512, 1024], P(None, 'tp'), may hold values from -0.25 to 0.25
- value_up: bfloat16 [512, 1024], P(None, 'tp'), may hold values from -2 to 2
- out_proj: bfloat16 [1024, 2048], replicated, may hold values from -0.1875 to 0.1875
- tokens: bfloat16 [2048, 2048], P(('ep', 'tp')), may hold values from -6 to 6
- moe_gain: float32 [2048], replicated, may hold values from 0.1 to 1.9
- routes: int32 [2048, 2], P(('ep', 'tp')), may hold values from 0 to 7, all different within a row; in each aligned block of 64 rows (0 to 63, 64 to 127, ...) at most 32 rows name the same one
- group_prob: float32 [2048], P(('ep', 'tp')), may hold values from 0.25 to 1
- expert_prob: float32 [2048, 2], P(('ep', 'tp')), may hold values from 0.02 to 1
- w_gate: bfloat16 [8, 2048, 1024], P('ep', None, 'tp'), may hold values from -0.125 to 0.125
- w_up: bfloat16 [8, 2048, 1024], P('ep', None, 'tp'), may hold values from -0.125 to 0.125
- w_down: bfloat16 [8, 1024, 2048], P('ep', 'tp'), may hold values from -0.1875 to 0.1875
Outputs:
- mixed: bfloat16 [1024, 2048], P(('ep', 'tp'))
- moe_out: bfloat16 [2048, 2048], P(('ep', 'tp'))
Inputs may be any that keep to these rules, and one draw needn't show every extreme that they name: `routes`: each row names 2 different experts; within the rows of one device no expert is named more than 32 times.
All inputs are finite; a program needn't handle non-finite values.
Results may differ from a plain program's by a relative error of at most 0.025.
Values may be sent and summed in bfloat16 or wider, within the bound.
A program may use at most 128 MiB of HBM per device.

v0:
```python
import math
import jax
import jax.numpy as jnp
from jax import lax
from jax.sharding import PartitionSpec as P

NOPE = 64
ROPE_DIM = 32
V_DIM = 64
epsilon = 1e-06
rope_base = 10000.0
masked_value = -1e30


def rms_scale(values, gain):
    widened = values.astype(jnp.float32)
    return widened * lax.rsqrt(jnp.mean(widened * widened, axis=-1, keepdims=True) + epsilon) * gain


def tables(positions, rope_width):
    half_width = rope_width // 2
    inverse = rope_base ** (-2.0 * jnp.arange(half_width, dtype=jnp.float32) / rope_width)
    angles = positions.astype(jnp.float32)[:, None] * inverse[None, :]
    return (jnp.cos(angles), jnp.sin(angles))


def rotate(values, cosine, sine):
    half_width = values.shape[-1] // 2
    lower = values[..., :half_width]
    upper = values[..., half_width:]
    return jnp.concatenate([lower * cosine - upper * sine, lower * sine + upper * cosine], axis=-1)


def keep_state(state_in):
    return state_in


def attend_block(running, query_rot, query_pos, key_part, value_part, rope_part):
    amount = key_part.shape[0]
    span_rows = math.gcd(amount, 1024)
    head_count = query_rot.shape[1]
    scale_factor = query_rot.shape[2] ** (-0.5)
    last_query = query_pos[-1]

    def update(state, block_at):
        row_begin = block_at * span_rows
        keys_here = lax.dynamic_slice_in_dim(key_part, row_begin, span_rows, 0).reshape(
            span_rows, head_count, -1
        )
        values_here = lax.dynamic_slice_in_dim(value_part, row_begin, span_rows, 0).reshape(
            span_rows, head_count, -1
        )
        rope_here = lax.dynamic_slice_in_dim(rope_part, row_begin, span_rows, 0)
        key_pos = row_begin + jnp.arange(span_rows, dtype=jnp.int32)

        def advance(state_in):
            top_old, totals, weighted = state_in
            shared = jnp.broadcast_to(
                rope_here[:, None, :], (span_rows, head_count, rope_here.shape[1])
            )
            full_keys = jnp.concatenate([keys_here, shared], axis=-1)
            scores = (
                jnp.einsum("qhd,khd->hqk", query_rot, full_keys, preferred_element_type=jnp.float32)
                * scale_factor
            )
            allowed = key_pos[None, :] <= query_pos[:, None]
            scores = jnp.where(allowed[None], scores, masked_value)
            top_new = jnp.maximum(top_old, jnp.max(scores, axis=-1))
            raised = jnp.where(allowed[None], jnp.exp(scores - top_new[..., None]), 0.0)
            factor = jnp.exp(top_old - top_new)
            totals = totals * factor + jnp.sum(raised, axis=-1)
            weighted = weighted * factor[..., None] + jnp.einsum(
                "hqk,khd->hqd",
                raised.astype(jnp.bfloat16),
                values_here,
                preferred_element_type=jnp.float32,
            )
            return (top_new, totals, weighted)

        return (lax.cond(key_pos[0] <= last_query, advance, keep_state, state), None)

    running, _ = lax.scan(update, running, jnp.arange(amount // span_rows))
    return running


def mixer_half(query, latent, rope_key, latent_gain, key_up, value_up, out_proj):
    query_rows = query.shape[0]
    own_rows = latent.shape[0]
    query_start = lax.axis_index("ep") * query_rows
    key_start = query_start + lax.axis_index("tp") * own_rows
    head_count = query.shape[1] // (NOPE + ROPE_DIM)
    normed = rms_scale(latent, latent_gain).astype(jnp.bfloat16)
    key_cos, key_sin = tables(key_start + jnp.arange(own_rows, dtype=jnp.int32), ROPE_DIM)
    rotated_key = rotate(rope_key.astype(jnp.float32), key_cos, key_sin).astype(jnp.bfloat16)
    query_pos = query_start + jnp.arange(query_rows, dtype=jnp.int32)
    query_cos, query_sin = tables(query_pos, ROPE_DIM)
    query_heads = query.reshape(query_rows, head_count, NOPE + ROPE_DIM)
    turned = rotate(
        query_heads[..., NOPE:].astype(jnp.float32), query_cos[:, None, :], query_sin[:, None, :]
    ).astype(jnp.bfloat16)
    query_rot = jnp.concatenate([query_heads[..., :NOPE], turned], axis=-1)
    last_query = query_start + query_rows - 1
    initial = (
        jnp.full((head_count, query_rows), masked_value, jnp.float32),
        jnp.zeros((head_count, query_rows), jnp.float32),
        jnp.zeros((head_count, query_rows, V_DIM), jnp.float32),
    )
    shard_rows = (
        lax.all_gather(normed, ("ep", "tp"), axis=0, tiled=True),
        lax.all_gather(rotated_key, ("ep", "tp"), axis=0, tiled=True),
    )

    def compute(state_in):
        key_part = jnp.dot(shard_rows[0], key_up, preferred_element_type=jnp.float32).astype(
            jnp.bfloat16
        )
        value_part = jnp.dot(shard_rows[0], value_up, preferred_element_type=jnp.float32).astype(
            jnp.bfloat16
        )
        return attend_block(state_in, query_rot, query_pos, key_part, value_part, shard_rows[1])

    running = lax.cond(jnp.int32(0) <= last_query, compute, keep_state, initial)
    totals = running[1]
    weighted = running[2]
    attention = (
        (weighted / totals[..., None])
        .transpose(1, 0, 2)
        .reshape(query_rows, head_count * V_DIM)
        .astype(jnp.bfloat16)
    )
    own_attention = lax.all_to_all(attention, "tp", split_axis=0, concat_axis=1, tiled=True)
    return jnp.dot(own_attention, out_proj, preferred_element_type=jnp.float32).astype(jnp.bfloat16)


def expert_half(tokens, moe_gain, routes, group_prob, expert_prob, w_gate, w_up, w_down):
    row_count, model_width = tokens.shape
    top_count = routes.shape[1]
    expert_count = lax.axis_size("ep")
    capacity = 2 * top_count * row_count // expert_count
    normed = rms_scale(tokens, moe_gain).astype(jnp.bfloat16)
    flat_routes = routes.reshape(-1)
    onehot = (flat_routes[:, None] == jnp.arange(expert_count, dtype=jnp.int32)[None, :]).astype(
        jnp.int32
    )
    earlier = jnp.cumsum(onehot, axis=0) - onehot
    slot_index = jnp.sum(earlier * onehot, axis=1)
    target = flat_routes * capacity + slot_index
    owner = target[None, :] == jnp.arange(expert_count * capacity, dtype=jnp.int32)[:, None]
    dispatch_table = jnp.any(
        owner.reshape(expert_count * capacity, row_count, top_count), axis=2
    ).astype(jnp.bfloat16)
    outgoing = jnp.dot(dispatch_table, normed, preferred_element_type=jnp.float32).astype(
        jnp.bfloat16
    )
    outgoing = outgoing.reshape(expert_count, capacity, model_width)
    arrived = lax.all_to_all(outgoing, "ep", split_axis=0, concat_axis=0, tiled=True)
    sources, slots, _ = arrived.shape
    flat_rows = arrived.reshape(sources * slots, model_width)
    shard_rows = lax.all_gather(flat_rows, "tp", axis=0, tiled=True)
    gate_values = jnp.dot(shard_rows, w_gate[0], preferred_element_type=jnp.float32)
    up_values = jnp.dot(shard_rows, w_up[0], preferred_element_type=jnp.float32)
    hidden = (jax.nn.silu(gate_values) * up_values).astype(jnp.bfloat16)

    def lower(offset, amount):
        return jnp.dot(hidden, w_down[0], preferred_element_type=jnp.float32)

    summed = lax.psum_scatter(
        lower(jnp.int32(0), sources * slots * lax.axis_size("tp")).astype(jnp.bfloat16),
        "tp",
        scatter_dimension=0,
        tiled=True,
    )
    result = summed.reshape(sources, slots, model_width)
    returned = lax.all_to_all(result, "ep", split_axis=0, concat_axis=0, tiled=True)
    returned_flat = returned.reshape(expert_count * capacity, model_width)
    picked = returned_flat[target].reshape(row_count, top_count, model_width).astype(jnp.float32)
    shares = group_prob[:, None] * expert_prob / jnp.sum(expert_prob, axis=1, keepdims=True)
    return jnp.sum(shares[:, :, None] * picked, axis=1).astype(jnp.bfloat16)


def body(
    query,
    latent,
    rope_key,
    latent_gain,
    key_up,
    value_up,
    out_proj,
    tokens,
    moe_gain,
    routes,
    group_prob,
    expert_prob,
    w_gate,
    w_up,
    w_down,
):
    mixed = mixer_half(query, latent, rope_key, latent_gain, key_up, value_up, out_proj)
    moe_out = expert_half(tokens, moe_gain, routes, group_prob, expert_prob, w_gate, w_up, w_down)
    return (mixed, moe_out)


def solution(mesh):
    return jax.shard_map(
        body,
        mesh=mesh,
        in_specs=(
            P("ep", "tp"),
            P(("ep", "tp"), None),
            P(("ep", "tp"), None),
            P(),
            P(None, "tp"),
            P(None, "tp"),
            P(),
            P(("ep", "tp"), None),
            P(),
            P(("ep", "tp"), None),
            P(("ep", "tp")),
            P(("ep", "tp"), None),
            P("ep", None, "tp"),
            P("ep", None, "tp"),
            P("ep", "tp", None),
        ),
        out_specs=(P(("ep", "tp"), None), P(("ep", "tp"), None)),
        check_vma=False,
    )
```

profile of v0, /device:TPU:0, one launch (start us, length us, event | category | flops | bytes accessed | tf_op | source)
XLA Modules:
  0.0 223.9 jit_solution(14774280976944361633)
XLA Ops:
  7.2 0.8 copy.68
  8.1 0.1 eq.29
  8.3 0.2 reduce_window_sum.11
  8.5 0.2 select_reduce_fusion
  8.7 0.1 reduce_sum.63
  8.8 0.6 broadcast_multiply_fusion
  9.6 1.1 fusion.27
  10.8 1.6 convolution_convert_fusion.3
  12.3 33.0 %all_to_all.26 = bf16[8,32,2048]{2,1,0:T(8,128)(2,1)} all-to-all(bf16[8,32,2048]{2,1,0:T(8,128)(2,1)S(1)} %bitcast.53), channel_id=1, replica_groups=mesh['ep'=8,'tp'=4] {'ep'}, dimensions={0} | all-to-all | bytes 2097152 | tf_op jit(solution)/shard_map/all_to_all | solution.py:156
  45.5 0.7 fusion.37
  46.3 32.6 %all-gather.5.cloned.1.call-done = bf16[1024,2048]{1,0:T(8,128)(2,1)} async-done(((bf16[256,2048]{1,0:T(8,128)(2,1)}), bf16[1024,2048]{1,0:T(8,128)(2,1)}) %all-gather.5.cloned.1.call-update) | async-done | bytes 4194320 | tf_op jit(solution)/shard_map/all_gather | solution.py:159
  78.9 4.4 %fusion.20 = f32[1024,256]{1,0:T(8,128)} fusion(bf16[1024,2048]{1,0:T(8,128)(2,1)} %all-gather.5.cloned.1.call-done, bf16[1,2048,256]{2,1,0:T(8,128)(2,1)S(1)} %copy-done.11), kind=kOutput, calls=%fused_computation.33 | convolution fusion | flops 1073741824 | bytes 6291456 | tf_op jit(solution)/shard_map/dot_general | solution.py:160
  83.3 8.8 %convolution_convert_fusion.2 = bf16[1024,2048]{1,0:T(8,128)(2,1)} fusion(bf16[1024,2048]{1,0:T(8,128)(2,1)} %all-gather.5.cloned.1.call-done, bf16[1,256,2048]{2,1,0:T(8,128)(2,1)S(1)} %copy-done, bf16[1,2048,256]{2,1,0:T(8,128)(2,1)S(1)} %copy-done.12, f32[1024,256]{1,0:T(8,128)} %fusion.20), kind=kOutput, calls=%fused_computation.26 | convolution fusion | flops 2151153664 | bytes 11534336 | tf_op jit(solution)/shard_map/dot_general | solution.py:165
  92.2 0.8 copy-done.6
  93.0 0.1 copy.63
  93.3 0.1 fusion.45
  93.5 41.5 %all_gather.10 = bf16[1024,32]{1,0:T(8,128)(2,1)S(1)} all-gather(bf16[32,32]{1,0:T(8,128)(2,1)S(1)} %copy.62), channel_id=1, replica_groups=mesh['ep'=8,'tp'=4] {'ep','tp'}, dimensions={0}, use_global_device_ids=true | all-gather | bytes 67584 | tf_op jit(solution)/shard_map/all_gather | solution.py:110
  135.0 0.1 multiply_cosine_fusion
  135.2 1.1 all-gather.3.cloned.1.call-done
  136.2 14.5 %conditional.2 = ((f32[4,128]{1,0:T(4,128)}, f32[4,128,64]{1,2,0:T(8,128)})) conditional(s32[]{:T(128)} %convert_element_type.90, () %tuple.32, (s32[]{:T(128)}, s32[128]{0:T(128)S(1)}, bf16[1024,512]{1,0:T(8,128)(2,1)}, bf16[512,256]{1,0:T(8,128)(2,1)S(1)}, bf16[512,256]{1,0:T(8,128)(2,1)S(1)}, /*index=5*/bf16[1024,32]{1,0:T(8,128)(2,1)S(1)}, ...), branch_computations={%region_1.0_spmd, %region_2.7_spmd} | conditional | flops 713754240 | bytes 23273134 | solution.py:122
  136.2 1.7 convolution_convert_fusion
  137.9 1.7 convolution_convert_fusion.1
  139.6 0.7 broadcast_in_dim.74
  140.3 0.5 broadcast_in_dim.55
  140.8 0.6 slice.18
  141.4 0.6 slice.17
  143.2 7.5 %conditional = ((f32[4,128]{1,0:T(4,128)}, f32[4,128,64]{1,2,0:T(8,128)})) conditional(s32[]{:T(128)} %bitcast.3, (f32[4,128]{1,0:T(4,128)}, f32[4,128,64]{1,2,0:T(8,128)}) %tuple.26, (s32[1024]{0:T(1024)S(1)}, s32[128]{0:T(128)S(1)}, bf16[1024,256]{1,0:T(8,128)(2,1)S(1)}, bf16[1024,32]{1,0:T(8,128)(2,1)S(1)}, bf16[128,4,96]{0,2,1:T(8,128)(2,1)S(1)}, ...), branch_computations={%region_3.3_spmd, %region_4.6_spmd} | conditional | flops 176358912 | bytes 19460660 | solution.py:80
  143.2 0.2 broadcast_compare_fusion
  143.4 0.2 copy.59
  143.6 0.1 copy.72
  143.8 0.6 fusion
  144.4 1.3 copy-done.1
  145.7 0.5 fusion.2
  146.3 1.2 subtract_exponential_fusion
  147.5 0.2 copy.60
  147.7 3.1 %convolution_add_fusion = f32[4,128,64]{1,2,0:T(8,128)} fusion(bf16[1024,4,64]{0,2,1:T(8,128)(2,1)S(1)} %bitcast.56, f32[4,1024,128]{2,1,0:T(8,128)} %copy-done.1, f32[4,128]{1,0:T(4,128)S(1)} %broadcast_maximum_fusion, pred[128,1024]{0,1:T(8,128)(4,1)S(1)} %broadcast_compare_fusion, f32[4,128,64]{1,2,0:T(8,128)} %get-tuple-element.110, ...), kind=kOutput, calls=%fused_computation.6 | convolution fusion | flops 69795840 | bytes 3018752 | tf_op jit(solution)/shard_map/cond/branch_1_fun/while/body/eval_jaxpr/cond/branch_1_fun/hqk,khd->hqd/dot_general | solution.py:72
  150.7 1.0 fusion.39
  151.7 0.1 copy.65
  151.8 0.1 convert_element_type.99
  152.0 6.6 %all_to_all.27 = bf16[4,32,256]{2,1,0:T(8,128)(2,1)S(1)} all-to-all(bf16[4,32,256]{2,1,0:T(8,128)(2,1)S(1)} %convert_element_type.99), channel_id=1, replica_groups=mesh['ep'=8,'tp'=4] {'tp'}, dimensions={0} | all-to-all | bytes 131072 | tf_op jit(solution)/shard_map/all_to_all | solution.py:131
  158.6 23.9 %reduce-scatter.2.cloned.1.call-done = bf16[256,2048]{1,0:T(8,128)(2,1)} async-done(((bf16[1024,2048]{1,0:T(8,128)(2,1)}), bf16[256,2048]{1,0:T(8,128)(2,1)}) %reduce-scatter.2.cloned.1.call-update) | async-done | bytes 1048592 | tf_op jit(solution)/shard_map/reduce_scatter | solution.py:167
  182.5 5.4 %all-to-all-start.2 = ((bf16[8,32,2048]{2,1,0:T(8,128)(2,1)}), bf16[8,32,2048]{2,1,0:T(8,128)(2,1)S(1)}, u32[]{:S(2)}, u32[]{:S(2)}) async-start(bf16[8,32,2048]{2,1,0:T(8,128)(2,1)} %bitcast.54), calls=%async_computation.3 | async-start | bytes 2097152 | tf_op jit(solution)/shard_map/all_to_all | solution.py:174
  187.9 0.1 mul.229
  188.2 3.7 %convolution_convert_fusion.4 = bf16[32,2048]{1,0:T(8,128)(2,1)} fusion(bf16[32,1024]{1,0:T(8,128)(2,1)S(1)} %bitcast.59, bf16[1024,2048]{1,0:T(8,128)(2,1)} %param.25), kind=kOutput, calls=%fused_computation.28 | convolution fusion | flops 134283264 | bytes 4390912 | tf_op jit(solution)/shard_map/dot_general | solution.py:132
  191.9 21.7 %all-to-all-done.2 = bf16[8,32,2048]{2,1,0:T(8,128)(2,1)S(1)} async-done(((bf16[8,32,2048]{2,1,0:T(8,128)(2,1)}), bf16[8,32,2048]{2,1,0:T(8,128)(2,1)S(1)}, u32[]{:S(2)}, u32[]{:S(2)}) %all-to-all-start.2) | async-done | bytes 1048608 | tf_op jit(solution)/shard_map/all_to_all | solution.py:174
  213.6 0.9 gather_fusion
  214.5 0.7 reshape.210
  215.2 2.2 multiply_reduce_fusion
  (59 shorter events, 1.0 us)
Async XLA Ops:
  7.2 76.2 %copy-start = (bf16[1,256,2048]{2,1,0:T(8,128)(2,1)S(1)}, bf16[1,256,2048]{2,1,0:T(8,128)(2,1)}, u32[]{:S(2)}) copy-start(bf16[1,256,2048]{2,1,0:T(8,128)(2,1)} %param.33) | copy-start | bytes 3145732
  7.2 71.8 %all-gather.5.cloned.1.call-start = ((), (), s32[]{:S(2)}) async-start(), calls=%async_computation.5 | async-start | bytes 5242880 | tf_op jit(solution)/shard_map/all_gather | solution.py:159
  10.7 34.6 %copy-start.4 = (bf16[32,512]{1,0:T(8,128)(2,1)S(1)}, bf16[32,512]{1,0:T(8,128)(2,1)}, u32[]{:S(2)}) copy-start(bf16[32,512]{1,0:T(8,128)(2,1)} %param.20) | copy-start | bytes 98308
  10.7 34.8 %copy-start.9 = (f32[512]{0:T(512)S(1)}, f32[512]{0:T(512)}, u32[]{:S(2)}) copy-start(f32[512]{0:T(512)} %param.22) | copy-start | bytes 6148
  10.8 68.2 %copy-start.11 = (bf16[1,2048,256]{2,1,0:T(8,128)(2,1)S(1)}, bf16[1,2048,256]{2,1,0:T(8,128)(2,1)}, u32[]{:S(2)}) copy-start(bf16[1,2048,256]{2,1,0:T(8,128)(2,1)} %param.31) | copy-start | bytes 3145732
  45.3 90.9 %all-gather.3.cloned.1.call-start = ((), (), s32[]{:S(2)}) async-start(), calls=%async_computation.4 | async-start | bytes 1081344 | tf_op jit(solution)/shard_map/all_gather | solution.py:109
  46.2 37.1 %copy-start.12 = (bf16[1,2048,256]{2,1,0:T(8,128)(2,1)S(1)}, bf16[1,2048,256]{2,1,0:T(8,128)(2,1)}, u32[]{:S(2)}) copy-start(bf16[1,2048,256]{2,1,0:T(8,128)(2,1)} %param.32) | copy-start | bytes 3145732
  46.2 136.3 %reduce-scatter.2.cloned.1.call-start = ((), (), s32[]{:S(2)}) async-start(), calls=%async_computation.6 | async-start | bytes 5242880 | tf_op jit(solution)/shard_map/reduce_scatter | solution.py:167
  92.1 0.9 copy-start.6
  92.1 1.0 copy-start.7
  92.1 44.1 %copy-start.2 = (bf16[512,256]{1,0:T(8,128)(2,1)S(1)}, bf16[512,256]{1,0:T(8,128)(2,1)}, u32[]{:S(2)}) copy-start(bf16[512,256]{1,0:T(8,128)(2,1)} %param.23) | copy-start | bytes 786436
  92.1 44.1 %copy-start.3 = (bf16[512,256]{1,0:T(8,128)(2,1)S(1)}, bf16[512,256]{1,0:T(8,128)(2,1)}, u32[]{:S(2)}) copy-start(bf16[512,256]{1,0:T(8,128)(2,1)} %param.24) | copy-start | bytes 786436
  144.4 1.3 copy-start.1
  150.7 37.2 %copy-start.5 = (s32[64,2]{1,0:T(8,128)S(1)}, s32[64,2]{1,0:T(8,128)}, u32[]{:S(2)}) copy-start(s32[64,2]{1,0:T(8,128)} %get-tuple-element.197) | copy-start | bytes 1540
  150.7 37.3 %copy-start.8 = (f32[64,2]{0,1:T(2,128)S(1)}, f32[64,2]{0,1:T(2,128)}, u32[]{:S(2)}) copy-start(f32[64,2]{0,1:T(2,128)} %param.30) | copy-start | bytes 1540
  150.7 37.4 %copy-start.10 = (f32[64]{0:T(128)S(1)}, f32[64]{0:T(128)}, u32[]{:S(2)}) copy-start(f32[64]{0:T(128)} %param.29) | copy-start | bytes 772
  182.5 31.1 %all-to-all-start.2 = ((bf16[8,32,2048]{2,1,0:T(8,128)(2,1)}), bf16[8,32,2048]{2,1,0:T(8,128)(2,1)S(1)}, u32[]{:S(2)}, u32[]{:S(2)}) async-start(bf16[8,32,2048]{2,1,0:T(8,128)(2,1)} %bitcast.54), calls=%async_computation.3 | async-start | bytes 2097152 | tf_op jit(solution)/shard_map/all_to_all | solution.py:174
Sparse Core Ops, SparseCore 0:
  45.4 33.4 all-gather.4
  82.4 53.8 all-gather.2
  138.8 43.6 reduce-scatter.1
where the time goes:
time: 225 us; the launch traced here: 224 us
  blocking collectives  81.1 us (36%)
  waiting for transfers between devices  79.3 us (35%)
  matrix products  25.4 us (11%)
  between operations  14 us (6%)
  local copies, waits for them, and re-layouts  8.74 us (4%)
  other arithmetic  8.56 us (4%)
  starting transfers between devices  5.53 us (2%)
    all_gather x1, blocking collectives, mixer_half(): lax.all_gather(rotated_key, ('ep', 'tp'), axis=0, tiled=True)  41.5 us
    all_to_all x1, blocking collectives, expert_half(): lax.all_to_all(outgoing, 'ep', split_axis=0, concat_axis=0, tiled=True)  33 us
    all_gather x1, waiting for transfers between devices, expert_half(): shard_rows = lax.all_gather(flat_rows, 'tp', axis=0, tiled=True)  32.6 us
    reduce_scatter x1, waiting for transfers between devices, expert_half(): lax.psum_scatter(lower(jnp.int32(0), sources * slots * lax.axis_size('tp'...  23.9 us
    all_to_all x1, waiting for transfers between devices, expert_half(): lax.all_to_all(result, 'ep', split_axis=0, concat_axis=0, tiled=True)  21.7 us
    dot_general x1, matrix products, lower(): return jnp.dot(hidden, w_down[0], preferred_element_type=jnp.float32)  8.77 us
    all_to_all x1, blocking collectives, mixer_half(): lax.all_to_all(attention, 'tp', split_axis=0, concat_axis=1, tiled=True)  6.64 us
    all_to_all x1, starting transfers between devices, expert_half(): lax.all_to_all(result, 'ep', split_axis=0, concat_axis=0, tiled=True)  5.41 us
  transfers between devices with their start and end apart: 4, of which 4 were waited for; matrix products, arithmetic and copies ran while one was open for 14% of the time, Pallas kernels for 0%

commit v1 on v0

--- a/solution.py
+++ b/solution.py
@@ -10,6 +10,16 @@
 epsilon = 1e-06
 rope_base = 10000.0
 masked_value = -1e30
+
+
+def gather_by_hops(x, name, along):
+    peers = lax.axis_size(name)
+    moving, blocks = (x, [x])
+    for _ in range(peers - 1):
+        moving = lax.ppermute(moving, name, [(i, (i + 1) % peers) for i in range(peers)])
+        blocks.insert(0, moving)
+    line = jnp.concatenate(blocks, axis=along)
+    return jnp.roll(line, (lax.axis_index(name) + 1) * x.shape[along], axis=along)
 
 
 def rms_scale(values, gain):
@@ -156,7 +166,7 @@
     arrived = lax.all_to_all(outgoing, "ep", split_axis=0, concat_axis=0, tiled=True)
     sources, slots, _ = arrived.shape
     flat_rows = arrived.reshape(sources * slots, model_width)
-    shard_rows = lax.all_gather(flat_rows, "tp", axis=0, tiled=True)
+    shard_rows = gather_by_hops(flat_rows, "tp", 0)
     gate_values = jnp.dot(shard_rows, w_gate[0], preferred_element_type=jnp.float32)
     up_values = jnp.dot(shard_rows, w_up[0], preferred_element_type=jnp.float32)
     hidden = (jax.nn.silu(gate_values) * up_values).astype(jnp.bfloat16)

time: 225 us -> 213 us (0.947)
  waiting for transfers between devices: 79.3 us -> 63.4 us
  local copies, waits for them, and re-layouts: 8.74 us -> 17.5 us
  matrix products: 25.4 us -> 21.8 us
    ppermute x0 -> x3, waiting for transfers between devices: none -> 42.4 us  [gather_by_hops(): lax.ppermute(moving, name, [(i, (i + 1) % peers) for i in range(peers)])]
    all_gather x1 -> x0, waiting for transfers between devices: 32.6 us -> none  [expert_half(): shard_rows = lax.all_gather(flat_rows, 'tp', axis=0, tiled=True)]
    reduce_scatter x1, waiting for transfers between devices: 23.9 us -> 0.01 us  [expert_half(): lax.psum_scatter(lower(jnp.int32(0), sources * slots * lax.axis_size('tp'...]
    unnamed x27 -> x32, local copies, waits for them, and re-layouts: 1.96 us -> 10.6 us
    dot_general x1, matrix products: 4.39 us -> 1.25 us  [expert_half(): up_values = jnp.dot(shard_rows, w_up[0], preferred_element_type=jnp.float32)]
  transfers between devices with their start and end apart: 4 -> 6, of which waited for: 4 -> 4; matrix products, arithmetic and copies ran while one was open for 14% -> 16% of each run, Pallas kernels for 0% -> 0%
where the time goes in v1:
time: 213 us; the launch traced here: 212 us
  blocking collectives  80.1 us (38%)
  waiting for transfers between devices  63.4 us (30%)
  matrix products  21.8 us (10%)
  local copies, waits for them, and re-layouts  17.5 us (8%)
  between operations  15.9 us (7%)
  other arithmetic  8.64 us (4%)
  starting transfers between devices  3.83 us (2%)
    ppermute x3, waiting for transfers between devices, gather_by_hops(): lax.ppermute(moving, name, [(i, (i + 1) % peers) for i in range(peers)])  42.4 us
    all_gather x1, blocking collectives, mixer_half(): lax.all_gather(rotated_key, ('ep', 'tp'), axis=0, tiled=True)  40.7 us
    all_to_all x1, blocking collectives, expert_half(): lax.all_to_all(outgoing, 'ep', split_axis=0, concat_axis=0, tiled=True)  32.9 us
    all_to_all x1, waiting for transfers between devices, expert_half(): lax.all_to_all(result, 'ep', split_axis=0, concat_axis=0, tiled=True)  21 us
    unnamed x32, local copies, waits for them, and re-layouts  10.6 us
    dot_general x1, matrix products, lower(): return jnp.dot(hidden, w_down[0], preferred_element_type=jnp.float32)  8.5 us
    all_to_all x1, blocking collectives, mixer_half(): lax.all_to_all(attention, 'tp', split_axis=0, concat_axis=1, tiled=True)  6.49 us
  transfers between devices with their start and end apart: 6, of which 4 were waited for; matrix products, arithmetic and copies ran while one was open for 16% of the time, Pallas kernels for 0%

profile of v1, /device:TPU:0, one launch (start us, length us, event | category | flops | bytes accessed | tf_op | source)
XLA Modules:
  0.0 212.5 jit_solution(13588335640509664730)
XLA Ops:
  8.1 0.8 copy.68
  8.9 0.1 eq.32
  9.2 0.2 reduce_window_sum.11
  9.3 0.2 select_reduce_fusion
  9.5 0.1 reduce_sum.63
  9.8 1.1 fusion.23
  11.0 1.5 convolution_convert_fusion.3
  12.4 32.9 %all_to_all.26 = bf16[8,32,2048]{2,1,0:T(8,128)(2,1)S(1)} all-to-all(bf16[8,32,2048]{2,1,0:T(8,128)(2,1)S(1)} %bitcast.56), channel_id=1, replica_groups=mesh['ep'=8,'tp'=4] {'ep'}, dimensions={0} | all-to-all | bytes 2097152 | tf_op jit(solution)/shard_map/all_to_all | solution.py:166
  45.3 14.2 %collective-permute-done = bf16[256,2048]{1,0:T(8,128)(2,1)S(1)} collective-permute-done((bf16[256,2048]{1,0:T(8,128)(2,1)S(1)}, bf16[256,2048]{1,0:T(8,128)(2,1)S(1)}, u32[]{:S(2)}, u32[]{:S(2)}) %collective-permute-start) | collective-permute-done | bytes 1048608 | tf_op jit(solution)/shard_map/ppermute | solution.py:19
  59.5 14.3 %collective-permute-done.1 = bf16[256,2048]{1,0:T(8,128)(2,1)} collective-permute-done((bf16[256,2048]{1,0:T(8,128)(2,1)S(1)}, bf16[256,2048]{1,0:T(8,128)(2,1)}, u32[]{:S(2)}, u32[]{:S(2)}) %collective-permute-start.1) | collective-permute-done | bytes 1048608 | tf_op jit(solution)/shard_map/ppermute | solution.py:19
  74.0 0.7 fusion.41
  74.8 13.9 %collective-permute-done.2 = bf16[256,2048]{1,0:T(8,128)(2,1)} collective-permute-done((bf16[256,2048]{1,0:T(8,128)(2,1)}, bf16[256,2048]{1,0:T(8,128)(2,1)}, u32[]{:S(2)}, u32[]{:S(2)}) %collective-permute-start.2) | collective-permute-done | bytes 1048608 | tf_op jit(solution)/shard_map/ppermute | solution.py:19
  88.7 1.3 constant_dynamic-update-slice_fusion.7
  89.9 1.3 constant_dynamic-update-slice_fusion.6
  91.4 1.4 constant_dynamic-update-slice_fusion.3
  92.8 1.3 constant_dynamic-update-slice_fusion.2
  94.3 3.2 %copy-done.4 = bf16[2048,2048]{1,0:T(8,128)(2,1)} copy-done((bf16[2048,2048]{1,0:T(8,128)(2,1)}, bf16[2048,2048]{1,0:T(8,128)(2,1)S(1)}, u32[]{:S(2)}) %copy-start.4) | copy-done | bytes 8388632
  97.5 1.2 fusion.16
  98.8 8.5 %convolution_convert_fusion.2 = bf16[1024,2048]{1,0:T(8,128)(2,1)} fusion(bf16[1,256,2048]{2,1,0:T(8,128)(2,1)S(1)} %copy-done, f32[1024,256]{1,0:T(8,128)S(1)} %fusion.16, bf16[2048,2048]{1,0:T(8,128)(2,1)} %copy-done.4, s32[]{:T(128)S(6)} %select_n.39, bf16[1,2048,256]{2,1,0:T(8,128)(2,1)S(1)} %copy-done.11), kind=kOutput, calls=%fused_computation.26 | convolution fusion | flops 2151153664 | bytes 11534340 | tf_op jit(solution)/shard_map/dot_general | solution.py:175
  107.3 0.9 copy-done.6
  108.7 40.7 %all_gather.7 = bf16[1024,32]{1,0:T(8,128)(2,1)S(1)} all-gather(bf16[32,32]{1,0:T(8,128)(2,1)S(1)} %copy.62), channel_id=1, replica_groups=mesh['ep'=8,'tp'=4] {'ep','tp'}, dimensions={0}, use_global_device_ids=true | all-gather | bytes 67584 | tf_op jit(solution)/shard_map/all_gather | solution.py:120
  149.6 14.5 %conditional.2 = ((f32[4,128]{1,0:T(4,128)}, f32[4,128,64]{1,2,0:T(8,128)})) conditional(s32[]{:T(128)} %convert_element_type.90, () %tuple.32, (s32[]{:T(128)}, s32[128]{0:T(128)S(1)}, bf16[1024,512]{1,0:T(8,128)(2,1)}, bf16[512,256]{1,0:T(8,128)(2,1)S(1)}, bf16[512,256]{1,0:T(8,128)(2,1)S(1)}, /*index=5*/bf16[1024,32]{1,0:T(8,128)(2,1)S(1)}, ...), branch_computations={%region_1.0_spmd, %region_2.7_spmd} | conditional | flops 713754240 | bytes 23273134 | solution.py:132
  149.6 1.7 convolution_convert_fusion
  151.3 1.7 convolution_convert_fusion.1
  153.0 0.7 broadcast_in_dim.74
  153.7 0.6 broadcast_in_dim.55
  154.3 0.6 slice.18
  154.9 0.5 slice.17
  156.6 7.5 %conditional = ((f32[4,128]{1,0:T(4,128)}, f32[4,128,64]{1,2,0:T(8,128)})) conditional(s32[]{:T(128)} %bitcast.3, (f32[4,128]{1,0:T(4,128)}, f32[4,128,64]{1,2,0:T(8,128)}) %tuple.26, (s32[1024]{0:T(1024)S(1)}, s32[128]{0:T(128)S(1)}, bf16[1024,256]{1,0:T(8,128)(2,1)S(1)}, bf16[1024,32]{1,0:T(8,128)(2,1)S(1)}, bf16[128,4,96]{0,2,1:T(8,128)(2,1)S(1)}, ...), branch_computations={%region_3.3_spmd, %region_4.6_spmd} | conditional | flops 176358912 | bytes 19460660 | solution.py:90
  156.7 0.2 broadcast_compare_fusion
  156.9 0.2 copy.59
  157.2 0.6 fusion
  157.9 1.3 copy-done.1
  159.2 0.5 fusion.2
  159.7 1.3 subtract_exponential_fusion
  161.0 0.2 copy.60
  161.2 2.9 %convolution_add_fusion = f32[4,128,64]{1,2,0:T(8,128)} fusion(bf16[1024,4,64]{0,2,1:T(8,128)(2,1)S(1)} %bitcast.59, f32[4,1024,128]{2,1,0:T(8,128)} %copy-done.1, f32[4,128]{1,0:T(4,128)S(1)} %broadcast_maximum_fusion, pred[128,1024]{0,1:T(8,128)(4,1)S(1)} %broadcast_compare_fusion, f32[4,128,64]{1,2,0:T(8,128)} %get-tuple-element.110, ...), kind=kOutput, calls=%fused_computation.6 | convolution fusion | flops 69795840 | bytes 3018752 | tf_op jit(solution)/shard_map/cond/branch_1_fun/while/body/eval_jaxpr/cond/branch_1_fun/hqk,khd->hqd/dot_general | solution.py:82
  164.1 0.9 fusion.43
  165.1 0.1 copy.65
  165.2 0.1 convert_element_type.99
  165.4 6.5 %all_to_all.27 = bf16[4,32,256]{2,1,0:T(8,128)(2,1)S(1)} all-to-all(bf16[4,32,256]{2,1,0:T(8,128)(2,1)S(1)} %convert_element_type.99), channel_id=1, replica_groups=mesh['ep'=8,'tp'=4] {'tp'}, dimensions={0} | all-to-all | bytes 131072 | tf_op jit(solution)/shard_map/all_to_all | solution.py:141
  171.8 3.7 %all-to-all-start.2 = ((bf16[8,32,2048]{2,1,0:T(8,128)(2,1)}), bf16[8,32,2048]{2,1,0:T(8,128)(2,1)S(1)}, u32[]{:S(2)}, u32[]{:S(2)}) async-start(bf16[8,32,2048]{2,1,0:T(8,128)(2,1)} %bitcast.57), calls=%async_computation.3 | async-start | bytes 2097152 | tf_op jit(solution)/shard_map/all_to_all | solution.py:184
  175.8 0.7 multiply_divide_fusion
  176.6 3.7 %convolution_convert_fusion.4 = bf16[32,2048]{1,0:T(8,128)(2,1)} fusion(bf16[32,1024]{1,0:T(8,128)(2,1)S(1)} %bitcast.62, bf16[1024,2048]{1,0:T(8,128)(2,1)} %param.25), kind=kOutput, calls=%fused_computation.32 | convolution fusion | flops 134283264 | bytes 4390912 | tf_op jit(solution)/shard_map/dot_general | solution.py:142
  180.2 21.0 %all-to-all-done.2 = bf16[8,32,2048]{2,1,0:T(8,128)(2,1)S(1)} async-done(((bf16[8,32,2048]{2,1,0:T(8,128)(2,1)}), bf16[8,32,2048]{2,1,0:T(8,128)(2,1)S(1)}, u32[]{:S(2)}, u32[]{:S(2)}) %all-to-all-start.2) | async-done | bytes 1048608 | tf_op jit(solution)/shard_map/all_to_all | solution.py:184
  201.2 0.9 gather_fusion
  202.1 0.7 reshape.210
  202.8 2.2 %multiply_reduce_fusion = bf16[64,2048]{1,0:T(8,128)(2,1)} fusion(f32[64,2,2048]{2,1,0:T(2,128)S(1)} %reshape.210, f32[64,2]{1,0:T(8,128)S(1)} %copy.67), kind=kLoop, calls=%fused_computation.36 | loop fusion | flops 393216 | bytes 1311232 | tf_op jit(solution)/shard_map/reduce_sum | solution.py:188
  (68 shorter events, 1.9 us)
Async XLA Ops:
  8.0 90.7 %copy-start = (bf16[1,256,2048]{2,1,0:T(8,128)(2,1)S(1)}, bf16[1,256,2048]{2,1,0:T(8,128)(2,1)}, u32[]{:S(2)}) copy-start(bf16[1,256,2048]{2,1,0:T(8,128)(2,1)} %param.33) | copy-start | bytes 3145732
  8.0 65.9 %copy-start.5 = (bf16[32,512]{1,0:T(8,128)(2,1)S(1)}, bf16[32,512]{1,0:T(8,128)(2,1)}, u32[]{:S(2)}) copy-start(bf16[32,512]{1,0:T(8,128)(2,1)} %param.20) | copy-start | bytes 98308
  8.0 66.0 %copy-start.9 = (f32[512]{0:T(512)S(1)}, f32[512]{0:T(512)}, u32[]{:S(2)}) copy-start(f32[512]{0:T(512)} %param.22) | copy-start | bytes 6148
  8.0 141.5 %all-gather.2.cloned.1.call-start = ((), (), s32[]{:S(2)}) async-start(), calls=%async_computation.4 | async-start | bytes 1081344 | tf_op jit(solution)/shard_map/all_gather | solution.py:119
  45.3 14.2 %collective-permute-start = (bf16[256,2048]{1,0:T(8,128)(2,1)S(1)}, bf16[256,2048]{1,0:T(8,128)(2,1)S(1)}, u32[]{:S(2)}, u32[]{:S(2)}) collective-permute-start(bf16[256,2048]{1,0:T(8,128)(2,1)S(1)} %bitcast.53), channel_id=1, source_target_pairs={{0,1},{1,2},{2,3},{3,0},{4,5},{5,6},{6,7},{7,4},{8,9},{9,10},{10,1... | collective-permute-start | bytes 3145736 | tf_op jit(solution)/shard_map/ppermute | solution.py:19
  59.5 14.3 %collective-permute-start.1 = (bf16[256,2048]{1,0:T(8,128)(2,1)S(1)}, bf16[256,2048]{1,0:T(8,128)(2,1)}, u32[]{:S(2)}, u32[]{:S(2)}) collective-permute-start(bf16[256,2048]{1,0:T(8,128)(2,1)S(1)} %collective-permute-done), channel_id=1, source_target_pairs={{0,1},{1,2},{2,3},{3,0},{4,5},{5,6},{6,7},{7,4},{8,9},{9,10},{10,1... | collective-permute-start | bytes 3145736 | tf_op jit(solution)/shard_map/ppermute | solution.py:19
  73.9 14.8 %collective-permute-start.2 = (bf16[256,2048]{1,0:T(8,128)(2,1)}, bf16[256,2048]{1,0:T(8,128)(2,1)}, u32[]{:S(2)}, u32[]{:S(2)}) collective-permute-start(bf16[256,2048]{1,0:T(8,128)(2,1)} %collective-permute-done.1), channel_id=1, source_target_pairs={{0,1},{1,2},{2,3},{3,0},{4,5},{5,6},{6,7},{7,4},{8,9},{9,10},{10,1... | collective-permute-start | bytes 3145736 | tf_op jit(solution)/shard_map/ppermute | solution.py:19
  74.7 97.1 %reduce-scatter.2.cloned.1.call-start = ((), (), s32[]{:S(2)}) async-start(), calls=%async_computation.5 | async-start | bytes 5242880 | tf_op jit(solution)/shard_map/reduce_scatter | solution.py:177
  91.4 6.1 %copy-start.10 = (bf16[1,2048,256]{2,1,0:T(8,128)(2,1)S(1)}, bf16[1,2048,256]{2,1,0:T(8,128)(2,1)}, u32[]{:S(2)}) copy-start(bf16[1,2048,256]{2,1,0:T(8,128)(2,1)} %param.32) | copy-start | bytes 3145732
  94.3 3.2 %copy-start.4 = (bf16[2048,2048]{1,0:T(8,128)(2,1)}, bf16[2048,2048]{1,0:T(8,128)(2,1)S(1)}, u32[]{:S(2)}) copy-start(bf16[2048,2048]{1,0:T(8,128)(2,1)S(1)} %constant_dynamic-update-slice_fusion) | copy-start | bytes 25165828
  97.5 1.3 copy-start.11
  107.3 0.9 copy-start.6
  107.3 1.0 copy-start.7
  107.3 42.3 %copy-start.2 = (bf16[512,256]{1,0:T(8,128)(2,1)S(1)}, bf16[512,256]{1,0:T(8,128)(2,1)}, u32[]{:S(2)}) copy-start(bf16[512,256]{1,0:T(8,128)(2,1)} %param.23) | copy-start | bytes 786436
  107.3 42.3 %copy-start.3 = (bf16[512,256]{1,0:T(8,128)(2,1)S(1)}, bf16[512,256]{1,0:T(8,128)(2,1)}, u32[]{:S(2)}) copy-start(bf16[512,256]{1,0:T(8,128)(2,1)} %param.24) | copy-start | bytes 786436
  149.6 26.1 %copy-start.8 = (f32[64,2]{0,1:T(2,128)S(1)}, f32[64,2]{0,1:T(2,128)}, u32[]{:S(2)}) copy-start(f32[64,2]{0,1:T(2,128)} %param.30) | copy-start | bytes 1540
  157.8 1.3 copy-start.1
  171.8 29.3 %all-to-all-start.2 = ((bf16[8,32,2048]{2,1,0:T(8,128)(2,1)}), bf16[8,32,2048]{2,1,0:T(8,128)(2,1)S(1)}, u32[]{:S(2)}, u32[]{:S(2)}) async-start(bf16[8,32,2048]{2,1,0:T(8,128)(2,1)} %bitcast.57), calls=%async_computation.3 | async-start | bytes 2097152 | tf_op jit(solution)/shard_map/all_to_all | solution.py:184
Sparse Core Ops, SparseCore 0:
  74.9 52.9 all-gather.1
Sparse Core Ops, SparseCore 1:
  107.4 44.6 reduce-scatter.1
